TPU v7x, 32 devices: a whole 2x2x4 slice. The times are simulated.
32 devices in a mesh: ep: 16 (over z, y, x), tp: 2 (over core).
Axes of the slice: x: 2, y: 2, z: 4, core: 2. Of those that a mesh axis runs over, the one named last changes fastest.
Arguments:
- tokens: bfloat16 [256, 2048], P('ep'), may hold values from -6 to 6
- norm_gain: bfloat16 [2048], replicated, may hold values from 0.099609375 to 1.8984375
- w_query: bfloat16 [2048, 512], P(None, 'tp'), may hold values from -0.125 to 0.125
- w_key: bfloat16 [2048, 256], P(None, 'tp'), may hold values from -0.125 to 0.125
- w_value: bfloat16 [2048, 256], P(None, 'tp'), may hold values from -0.125 to 0.125
- w_forget: bfloat16 [2048, 8], P(None, 'tp'), may hold values from -0.25 to 0.25
- w_out: bfloat16 [512, 2048], P('tp'), may hold values from -0.25 to 0.25
- cache_keys: bfloat16 [256, 1024, 256], P('ep', None, 'tp'), may hold values from -700 to 700
- cache_values: bfloat16 [256, 1024, 256], P('ep', None, 'tp'), may hold values from -6 to 6
- cache_gates: float32 [256, 8, 1024], P('ep', 'tp'), as said below
- lengths: int32 [256], P('ep'), may hold values from 1 to 1024, as said below
- ffn_gain: bfloat16 [2048], replicated, may hold values from 0.099609375 to 1.8984375
- router_w: bfloat16 [2048, 16], replicated, may hold values from -0.125 to 0.125
- routes: int32 [256, 6], P('ep'), may hold values from 0 to 15, all different within a row; in each aligned block of 16 rows (0 to 15, 16 to 31, ...) at most 12 rows name the same one
- shared_gate: bfloat16 [2048, 512], P(None, 'tp'), may hold values from -0.125 to 0.125
- shared_up: bfloat16 [2048, 512], P(None, 'tp'), may hold values from -0.125 to 0.125
- shared_down: bfloat16 [512, 2048], P('tp'), may hold values from -0.25 to 0.25
- expert_gate: bfloat16 [16, 2048, 512], P('ep', None, 'tp'), may hold values from -0.125 to 0.125
- expert_up: bfloat16 [16, 2048, 512], P('ep', None, 'tp'), may hold values from -0.125 to 0.125
- expert_down: bfloat16 [16, 512, 2048], P('ep', 'tp'), may hold values from -0.25 to 0.25
Outputs:
- layer_out: bfloat16 [256, 2048], P('ep')
Inputs may be any that keep to these rules, and one draw needn't show every extreme that they name: `routes`: each row names 6 different experts. Among the rows of one index of ep no expert is named by more than 12 rows, and in every draw some expert is named by exactly 12 of them. `lengths`: in every draw some sequence has all 1024 positions. `cache_gates`: each row is non-increasing along the positions.
All inputs are finite; a program needn't handle non-finite values.
Results may differ from a plain program's by a relative error of at most 0.017.
Values may be sent and summed in bfloat16 or wider, within the bound.
A program may use at most 64 MiB of HBM per device.

v0:
```python
import jax
import jax.numpy as jnp
from jax import lax
from jax.sharding import PartitionSpec as P

HEAD_DIM = 64
EPS = 1e-06
ROUTE_SCALE = 2.5


def norm_rows(rows, norm_gain):
    values = rows.astype(jnp.float32)
    factor = lax.rsqrt(jnp.mean(values * values, axis=-1, keepdims=True) + EPS)
    return (values * factor * norm_gain.astype(jnp.float32)).astype(jnp.bfloat16)


def swiglu_hidden(rows, w_gate, w_up):
    gate_proj = jnp.dot(rows, w_gate, preferred_element_type=jnp.float32)
    upward = jnp.dot(rows, w_up, preferred_element_type=jnp.float32)
    return (jax.nn.silu(gate_proj) * upward).astype(jnp.bfloat16)


def route_weights(rows, router_w, chosen):
    scores = jax.nn.sigmoid(jnp.dot(rows, router_w, preferred_element_type=jnp.float32))
    picked = jnp.take_along_axis(scores, chosen, axis=1)
    return ROUTE_SCALE * picked / jnp.sum(picked, axis=1, keepdims=True)


def slot_hidden(incoming, expert_gate, expert_up):
    gate_proj = jnp.einsum(
        "scd,df->scf", incoming, expert_gate[0], preferred_element_type=jnp.float32
    )
    upward = jnp.einsum("scd,df->scf", incoming, expert_up[0], preferred_element_type=jnp.float32)
    return (jax.nn.silu(gate_proj) * upward).astype(jnp.bfloat16)


def attend(
    normed, w_query, w_key, w_value, w_forget, cache_keys, cache_values, cache_gates, lengths
):
    seq_count = normed.shape[0]
    head_count = w_forget.shape[1]
    kv_count = w_key.shape[1] // HEAD_DIM
    group_size = head_count // kv_count
    cache_len = cache_keys.shape[1]
    score_scale = HEAD_DIM ** (-0.5)
    queries = jnp.dot(normed, w_query, preferred_element_type=jnp.float32).astype(jnp.bfloat16)
    queries = queries.reshape(seq_count, kv_count, group_size, HEAD_DIM)
    key_new = jnp.dot(normed, w_key, preferred_element_type=jnp.float32).astype(jnp.bfloat16)
    key_new = key_new.reshape(seq_count, kv_count, HEAD_DIM)
    value_new = jnp.dot(normed, w_value, preferred_element_type=jnp.float32).astype(jnp.bfloat16)
    value_new = value_new.reshape(seq_count, kv_count, HEAD_DIM)
    log_gate = jax.nn.log_sigmoid(jnp.dot(normed, w_forget, preferred_element_type=jnp.float32))
    cached_keys = cache_keys.reshape(seq_count, cache_len, kv_count, HEAD_DIM)
    cached_values = cache_values.reshape(seq_count, cache_len, kv_count, HEAD_DIM)
    past_score = (
        jnp.einsum("skgd,slkd->skgl", queries, cached_keys, preferred_element_type=jnp.float32)
        * score_scale
    )
    last_index = jnp.broadcast_to((lengths - 1)[:, None, None], (seq_count, head_count, 1))
    last_gate = jnp.take_along_axis(cache_gates, last_index, axis=2)
    gate_bias = last_gate + log_gate[:, :, None] - cache_gates
    past_score = past_score + gate_bias.reshape(seq_count, kv_count, group_size, cache_len)
    is_valid = jnp.arange(cache_len)[None, :] < lengths[:, None]
    past_score = jnp.where(is_valid[:, None, None, :], past_score, -jnp.inf)
    self_score = (
        jnp.einsum("skgd,skd->skg", queries, key_new, preferred_element_type=jnp.float32)
        * score_scale
    )
    peak_score = jnp.maximum(jnp.max(past_score, axis=-1), self_score)
    past_weight = jnp.exp(past_score - peak_score[..., None])
    self_weight = jnp.exp(self_score - peak_score)
    weight_sum = jnp.sum(past_weight, axis=-1) + self_weight
    past_prob = (past_weight / weight_sum[..., None]).astype(jnp.bfloat16)
    self_prob = (self_weight / weight_sum).astype(jnp.bfloat16)
    mixed_heads = jnp.einsum(
        "skgl,slkd->skgd", past_prob, cached_values, preferred_element_type=jnp.float32
    )
    mixed_heads = (
        mixed_heads
        + self_prob.astype(jnp.float32)[..., None] * value_new.astype(jnp.float32)[:, :, None, :]
    )
    return mixed_heads.astype(jnp.bfloat16).reshape(seq_count, head_count * HEAD_DIM)


def per_device(
    tokens,
    norm_gain,
    w_query,
    w_key,
    w_value,
    w_forget,
    w_out,
    cache_keys,
    cache_values,
    cache_gates,
    lengths,
    ffn_gain,
    router_w,
    routes,
    shared_gate,
    shared_up,
    shared_down,
    expert_gate,
    expert_up,
    expert_down,
):
    seq_count = tokens.shape[0]
    width = tokens.shape[1]
    top_k = routes.shape[1]
    groups = lax.axis_size("ep")
    capacity = max(2, 2 * seq_count * top_k // groups)
    normed = norm_rows(tokens, norm_gain)
    attn = attend(
        normed, w_query, w_key, w_value, w_forget, cache_keys, cache_values, cache_gates, lengths
    )
    partial_value = jnp.dot(attn, w_out, preferred_element_type=jnp.float32)
    attended = lax.psum(partial_value.astype(jnp.bfloat16), "tp").astype(jnp.float32)
    residual_rows = (tokens.astype(jnp.float32) + attended).astype(jnp.bfloat16)
    ffn_rows = norm_rows(residual_rows, ffn_gain)
    shared_part = jnp.dot(
        swiglu_hidden(ffn_rows, shared_gate, shared_up),
        shared_down,
        preferred_element_type=jnp.float32,
    )
    flat_routes = routes.reshape(-1)
    expert_marks = (flat_routes[:, None] == jnp.arange(groups, dtype=jnp.int32)[None, :]).astype(
        jnp.int32
    )
    before = jnp.cumsum(expert_marks, axis=0) - expert_marks
    slot_rank = jnp.sum(before * expert_marks, axis=1)
    target = flat_routes * capacity + slot_rank
    sources = jnp.repeat(ffn_rows, top_k, axis=0)
    outgoing = jnp.zeros((groups * capacity, width), jnp.bfloat16).at[target].set(sources)
    outgoing = outgoing.reshape(groups, capacity, width)
    weights = route_weights(ffn_rows, router_w, routes)
    shared = lax.psum(shared_part.astype(jnp.bfloat16), "tp").astype(jnp.float32)
    hidden = slot_hidden(
        lax.all_to_all(outgoing, "ep", split_axis=0, concat_axis=0, tiled=True),
        expert_gate,
        expert_up,
    )
    part_rows = jnp.einsum(
        "scf,fd->scd", hidden, expert_down[0], preferred_element_type=jnp.float32
    )
    merged = lax.psum(part_rows.astype(jnp.bfloat16), "tp")
    returned = lax.all_to_all(merged, "ep", split_axis=0, concat_axis=0, tiled=True)
    answers = returned.reshape(groups * capacity, width)[target].astype(jnp.float32)
    routed = jnp.sum((answers * weights.reshape(-1, 1)).reshape(seq_count, top_k, width), axis=1)
    return (residual_rows.astype(jnp.float32) + shared + routed).astype(jnp.bfloat16)


def solution(mesh):
    placed = (
        P("ep", None),
        P(),
        P(None, "tp"),
        P(None, "tp"),
        P(None, "tp"),
        P(None, "tp"),
        P("tp", None),
        P("ep", None, "tp"),
        P("ep", None, "tp"),
        P("ep", "tp", None),
        P("ep"),
        P(),
        P(),
        P("ep", None),
        P(None, "tp"),
        P(None, "tp"),
        P("tp", None),
        P("ep", None, "tp"),
        P("ep", None, "tp"),
        P("ep", "tp", None),
    )
    return jax.shard_map(
        per_device, mesh=mesh, in_specs=placed, out_specs=P("ep", None), check_vma=False
    )
```

profile of v0, /device:TPU:8, one launch (start us, length us, event | category | flops | bytes accessed | tf_op | source)
XLA Modules:
  0.0 159.0 jit_solution(10485260314686976867)
XLA Ops:
  6.5 0.7 broadcast_add_fusion
  7.3 0.7 broadcast_compare_fusion
  7.9 0.7 iota_compare_fusion
  9.0 2.0 %gather_fusion.1 = f32[64]{0:T(128)S(1)} fusion(f32[16,4,1024]{2,1,0:T(4,128)} %param.29, s32[64]{0:T(128)S(1)} %reshape.274), kind=kCustom, calls=%fused_computation.1 | custom fusion | bytes 1280 | tf_op jit(solution)/shard_map/jit(take_along_axis)/gather | solution.py:60
  12.0 0.3 convolution_convert_fusion.3
  12.4 6.5 %copy.41 = bf16[16,1024,128]{1,2,0:T(8,128)(2,1)} copy(bf16[16,1024,128]{2,1,0:T(8,128)(2,1)} %param.27) | data formatting | bytes 8388608 | tf_op args[7]
  19.4 3.0 %fusion.55 = (f32[16,2,2]{2,1,0:T(2,128)S(1)}, f32[16,2,2,1024]{3,2,1,0:T(2,128)S(1)}) fusion(f32[16,2,2,1024]{3,2,1,0:T(2,128)S(1)} %reshape.254, bf16[16,2,2,64]{3,2,1,0:T(2,128)(2,1)S(1)} %reshape.252, bf16[16,1024,2,64]{1,3,2,0:T(8,128)(2,1)} %bitcast.50, pred[16,1024]{1,0:T(8,128)(4,1)S(1)} %iota_compare_fusion), kind=kOutput, calls=%fused_computation.103 | convolution fusion | flops 8650688 | bytes 4743424 | tf_op jit(solution)/shard_map/skgd,slkd->skgl/dot_general | solution.py:56
  22.4 0.3 fusion.16
  22.8 0.2 fusion.7
  23.1 6.4 %copy.45 = bf16[16,1024,128]{1,2,0:T(8,128)(2,1)} copy(bf16[16,1024,128]{2,1,0:T(8,128)(2,1)} %param.28) | data formatting | bytes 8388608 | tf_op args[8]
  29.5 3.5 %fusion.2 = bf16[16,2,2,64]{3,2,1,0:T(2,128)(2,1)S(1)} fusion(bf16[16,1024,2,64]{1,3,2,0:T(8,128)(2,1)} %bitcast.51, f32[16,2,2,1024]{3,2,1,0:T(2,128)S(1)} %get-tuple-element.12, f32[16,2,2]{2,1,0:T(2,128)S(1)} %get-tuple-element.8, f32[16,2,2]{2,1,0:T(2,128)S(1)} %multiply_maximum_fusion, f32[16,2,64]{2,1,0:T(2,128)S(1)} %reshape.262, ...), kind=kOutput, calls=%fused_computation.11 | convolution fusion | flops 8597504 | bytes 4473600 | tf_op jit(solution)/shard_map/skgl,slkd->skgd/dot_general | solution.py:75
  33.1 0.9 convolution_convert_fusion.2
  34.8 18.5 %all-reduce.4.cloned.1.call-done = bf16[16,2048]{1,0:T(8,128)(2,1)} async-done(((bf16[16,2048]{1,0:T(8,128)(2,1)}), bf16[16,2048]{1,0:T(8,128)(2,1)}) %all-reduce.4.cloned.1.call-update) | async-done | bytes 65552 | tf_op jit(solution)/shard_map/psum | solution.py:117
  53.4 1.0 fusion.21
  54.3 0.9 fusion.23
  55.5 1.4 scatter_custom_fusion
  56.9 1.2 reshape.259
  58.1 7.0 %all-to-all-start = ((bf16[16,12,2048]{2,1,0:T(8,128)(2,1)}), bf16[16,12,2048]{2,1,0:T(8,128)(2,1)S(1)}, u32[]{:S(2)}, u32[]{:S(2)}) async-start(bf16[16,12,2048]{2,1,0:T(8,128)(2,1)} %reshape.259), calls=%async_computation | async-start | bytes 2097152 | tf_op jit(solution)/shard_map/all_to_all | solution.py:138
  65.1 1.5 fusion.57
  66.6 2.9 %convolution_convert_fusion.1 = bf16[16,2048]{1,0:T(8,128)(2,1)} fusion(bf16[256,2048]{1,0:T(8,128)(2,1)} %param.36, bf16[16,2048]{1,0:T(8,128)(2,1)S(1)} %fusion.23, bf16[2048,256]{1,0:T(8,128)(2,1)} %param.35, f32[16,256]{1,0:T(8,128)S(1)} %fusion.57), kind=kOutput, calls=%fused_computation.5 | convolution fusion | flops 33611776 | bytes 2244608 | tf_op jit(solution)/shard_map/dot_general | solution.py:120
  69.5 21.4 %all-to-all-done = bf16[16,12,2048]{2,1,0:T(8,128)(2,1)S(1)} async-done(((bf16[16,12,2048]{2,1,0:T(8,128)(2,1)}), bf16[16,12,2048]{2,1,0:T(8,128)(2,1)S(1)}, u32[]{:S(2)}, u32[]{:S(2)}) %all-to-all-start) | async-done | bytes 786464 | tf_op jit(solution)/shard_map/all_to_all | solution.py:138
  90.9 1.7 %fusion.11 = f32[16,12,256]{2,1,0:T(8,128)S(1)} fusion(bf16[16,12,2048]{2,1,0:T(8,128)(2,1)S(1)} %all-to-all-done, bf16[1,2048,256]{2,1,0:T(8,128)(2,1)} %param.37), kind=kOutput, calls=%fused_computation.26 | convolution fusion | flops 201326592 | bytes 2031616 | tf_op jit(solution)/shard_map/scd,df->scf/dot_general | solution.py:30
  92.6 1.7 %fusion.9 = f32[16,12,256]{2,1,0:T(8,128)S(1)} fusion(bf16[16,12,2048]{2,1,0:T(8,128)(2,1)S(1)} %all-to-all-done, bf16[1,2048,256]{2,1,0:T(8,128)(2,1)} %param.38), kind=kOutput, calls=%fused_computation.24 | convolution fusion | flops 201326592 | bytes 2031616 | tf_op jit(solution)/shard_map/scd,df->scf/dot_general | solution.py:33
  94.3 1.5 convolution_convert_fusion
  95.8 18.8 %all-reduce.6.cloned.1.call-done = (bf16[16,12,2048]{2,0,1:T(8,128)(2,1)}, bf16[16,2048]{1,0:T(8,128)(2,1)}) async-done(((bf16[16,12,2048]{2,0,1:T(8,128)(2,1)}, bf16[16,2048]{1,0:T(8,128)(2,1)}), (bf16[16,12,2048]{2,0,1:T(8,128)(2,1)}, bf16[16,2048]{1,0:T(8,128)(2,1)})) %all-reduce.6.cloned.1.call-update) | async-done | bytes 851984 | tf_op jit(solution)/shard_map/psum | solution.py:145
  114.6 2.6 %copy.50 = bf16[16,12,2048]{2,1,0:T(8,128)(2,1)} copy(bf16[16,12,2048]{2,0,1:T(8,128)(2,1)} %get-tuple-element.5) | data formatting | bytes 1572864 | tf_op jit(solution)/shard_map/psum | solution.py:145
  117.1 7.0 %all-to-all-start.1 = ((bf16[16,12,2048]{2,1,0:T(8,128)(2,1)}), bf16[16,12,2048]{2,1,0:T(8,128)(2,1)S(1)}, u32[]{:S(2)}, u32[]{:S(2)}) async-start(bf16[16,12,2048]{2,1,0:T(8,128)(2,1)} %copy.50), calls=%async_computation.1 | async-start | bytes 2097152 | tf_op jit(solution)/shard_map/all_to_all | solution.py:146
  124.5 1.3 gather_fusion.2
  126.1 23.9 %all-to-all-done.1 = bf16[16,12,2048]{2,1,0:T(8,128)(2,1)S(1)} async-done(((bf16[16,12,2048]{2,1,0:T(8,128)(2,1)}), bf16[16,12,2048]{2,1,0:T(8,128)(2,1)S(1)}, u32[]{:S(2)}, u32[]{:S(2)}) %all-to-all-start.1) | async-done | bytes 786464 | tf_op jit(solution)/shard_map/all_to_all | solution.py:146
  150.1 0.8 gather_fusion
  151.1 0.4 multiply_reduce_fusion
  151.5 0.7 fusion.25
  (81 shorter events, 3.9 us)
Async XLA Ops:
  6.5 87.7 %copy-start = (bf16[1,256,2048]{2,1,0:T(8,128)(2,1)S(1)}, bf16[1,256,2048]{2,1,0:T(8,128)(2,1)}, u32[]{:S(2)}) copy-start(bf16[1,256,2048]{2,1,0:T(8,128)(2,1)} %param.39) | copy-start | bytes 3145732
  6.5 46.8 %all-reduce.4.cloned.1.call-start = ((), (), s32[]{:S(2)}) async-start(), calls=%async_computation.2 | async-start | bytes 131072 | tf_op jit(solution)/shard_map/psum | solution.py:117
  8.9 2.3 %copy-start.10 = (bf16[2048]{0:T(1024)(128)(2,1)S(1)}, bf16[2048]{0:T(1024)(128)(2,1)}, u32[]{:S(2)}) copy-start(bf16[2048]{0:T(1024)(128)(2,1)} %param.21) | copy-start | bytes 12292
  8.9 2.3 %copy-start.2 = (bf16[16,2048]{1,0:T(8,128)(2,1)S(1)}, bf16[16,2048]{1,0:T(8,128)(2,1)}, u32[]{:S(2)}) copy-start(bf16[16,2048]{1,0:T(8,128)(2,1)} %param.20) | copy-start | bytes 196612
  8.9 2.4 %copy-start.13 = (bf16[2048,4]{0,1:T(4,128)(2,1)S(1)}, bf16[2048,4]{0,1:T(4,128)(2,1)}, u32[]{:S(2)}) copy-start(bf16[2048,4]{0,1:T(4,128)(2,1)} %param.25) | copy-start | bytes 49156
  9.0 2.7 %copy-start.1 = (f32[16,4,1024]{2,1,0:T(4,128)S(1)}, f32[16,4,1024]{2,1,0:T(4,128)}, u32[]{:S(2)}) copy-start(f32[16,4,1024]{2,1,0:T(4,128)} %param.29) | copy-start | bytes 786436
  9.0 3.0 %copy-start.3 = (bf16[2048,256]{1,0:T(8,128)(2,1)S(1)}, bf16[2048,256]{1,0:T(8,128)(2,1)}, u32[]{:S(2)}) copy-start(bf16[2048,256]{1,0:T(8,128)(2,1)} %param.22) | copy-start | bytes 3145732
  12.4 6.5 %copy-start.6 = (bf16[2048,128]{1,0:T(8,128)(2,1)S(1)}, bf16[2048,128]{1,0:T(8,128)(2,1)}, u32[]{:S(2)}) copy-start(bf16[2048,128]{1,0:T(8,128)(2,1)} %param.23) | copy-start | bytes 1572868
  18.9 3.9 %copy-start.7 = (bf16[2048,128]{1,0:T(8,128)(2,1)S(1)}, bf16[2048,128]{1,0:T(8,128)(2,1)}, u32[]{:S(2)}) copy-start(bf16[2048,128]{1,0:T(8,128)(2,1)} %param.24) | copy-start | bytes 1572868
  29.5 3.6 %copy-start.4 = (bf16[256,2048]{1,0:T(8,128)(2,1)S(1)}, bf16[256,2048]{1,0:T(8,128)(2,1)}, u32[]{:S(2)}) copy-start(bf16[256,2048]{1,0:T(8,128)(2,1)} %param.26) | copy-start | bytes 3145732
  29.5 4.5 %copy-start.8 = (s32[16,6]{0,1:T(8,128)S(1)}, s32[16,6]{0,1:T(8,128)}, u32[]{:S(2)}) copy-start(s32[16,6]{0,1:T(8,128)} %param.33) | copy-start | bytes 1156
  29.5 5.3 %copy-start.11 = (bf16[2048]{0:T(1024)(128)(2,1)S(1)}, bf16[2048]{0:T(1024)(128)(2,1)}, u32[]{:S(2)}) copy-start(bf16[2048]{0:T(1024)(128)(2,1)} %param.31) | copy-start | bytes 12292
  58.1 32.8 %all-to-all-start = ((bf16[16,12,2048]{2,1,0:T(8,128)(2,1)}), bf16[16,12,2048]{2,1,0:T(8,128)(2,1)S(1)}, u32[]{:S(2)}, u32[]{:S(2)}) async-start(bf16[16,12,2048]{2,1,0:T(8,128)(2,1)} %reshape.259), calls=%async_computation | async-start | bytes 2097152 | tf_op jit(solution)/shard_map/all_to_all | solution.py:138
  65.1 49.5 %all-reduce.6.cloned.1.call-start = ((), (), s32[]{:S(2)}) async-start(), calls=%async_computation.3 | async-start | bytes 1703936 | tf_op jit(solution)/shard_map/psum | solution.py:145
  92.6 31.8 %copy-start.12 = (bf16[2048,16]{0,1:T(8,128)(2,1)S(1)}, bf16[2048,16]{0,1:T(8,128)(2,1)}, u32[]{:S(2)}) copy-start(bf16[2048,16]{0,1:T(8,128)(2,1)} %param.32) | copy-start | bytes 196612
  117.1 32.8 %all-to-all-start.1 = ((bf16[16,12,2048]{2,1,0:T(8,128)(2,1)}), bf16[16,12,2048]{2,1,0:T(8,128)(2,1)S(1)}, u32[]{:S(2)}, u32[]{:S(2)}) async-start(bf16[16,12,2048]{2,1,0:T(8,128)(2,1)} %copy.50), calls=%async_computation.1 | async-start | bytes 2097152 | tf_op jit(solution)/shard_map/all_to_all | solution.py:146
  125.8 25.7 %copy-start.5 = (bf16[16,2048]{1,0:T(8,128)(2,1)S(1)}, bf16[16,2048]{1,0:T(8,128)(2,1)}, u32[]{:S(2)}) copy-start(bf16[16,2048]{1,0:T(8,128)(2,1)} %all-reduce.4.cloned.1.call-done) | copy-start | bytes 196612
  125.8 25.7 %copy-start.9 = (bf16[16,2048]{1,0:T(8,128)(2,1)S(1)}, bf16[16,2048]{1,0:T(8,128)(2,1)}, u32[]{:S(2)}) copy-start(bf16[16,2048]{1,0:T(8,128)(2,1)} %get-tuple-element.6) | copy-start | bytes 196612
Sparse Core Ops, SparseCore 0:
  34.1 19.1 all-reduce.3
  95.9 18.6 all-reduce.5
where the time goes:
time: 160 us; the launch traced here: 159 us
  waiting for transfers between devices  82.6 us (52%)
  local copies, waits for them, and re-layouts  24.5 us (15%)
  matrix products  17.9 us (11%)
  starting transfers between devices  14 us (9%)
  between operations  13.8 us (9%)
  other arithmetic  6.22 us (4%)
    all_to_all x1, waiting for transfers between devices, per_device(): lax.all_to_all(merged, 'ep', split_axis=0, concat_axis=0, tiled=True)  23.9 us
    all_to_all x1, waiting for transfers between devices, per_device(): lax.all_to_all(outgoing, 'ep', split_axis=0, concat_axis=0, tiled=True)  21.4 us
    psum x1, waiting for transfers between devices, per_device(): merged = lax.psum(part_rows.astype(jnp.bfloat16), 'tp')  18.8 us
    psum x1, waiting for transfers between devices, per_device(): lax.psum(partial_value.astype(jnp.bfloat16), 'tp').astype(jnp.float32)  18.5 us
    unnamed x33, local copies, waits for them, and re-layouts  13 us
    all_to_all x1, starting transfers between devices, per_device(): lax.all_to_all(outgoing, 'ep', split_axis=0, concat_axis=0, tiled=True)  6.97 us
    all_to_all x1, starting transfers between devices, per_device(): lax.all_to_all(merged, 'ep', split_axis=0, concat_axis=0, tiled=True)  6.97 us
    dot_general x1, matrix products, attend(): jnp.einsum('skgl,slkd->skgd', past_prob, cached_values, preferred_element...  3.52 us
  transfers between devices with their start and end apart: 4, of which 4 were waited for; matrix products, arithmetic and copies ran while one was open for 4% of the time, Pallas kernels for 0%

commit v1 on v0

--- a/solution.py
+++ b/solution.py
@@ -114,7 +114,9 @@
         normed, w_query, w_key, w_value, w_forget, cache_keys, cache_values, cache_gates, lengths
     )
     partial_value = jnp.dot(attn, w_out, preferred_element_type=jnp.float32)
-    attended = lax.psum(partial_value.astype(jnp.bfloat16), "tp").astype(jnp.float32)
+    attended = jnp.sum(lax.all_gather(partial_value.astype(jnp.bfloat16), "tp"), axis=0).astype(
+        jnp.float32
+    )
     residual_rows = (tokens.astype(jnp.float32) + attended).astype(jnp.bfloat16)
     ffn_rows = norm_rows(residual_rows, ffn_gain)
     shared_part = jnp.dot(

time: 160 us -> 142 us (0.89)
  waiting for transfers between devices: 82.6 us -> 63.8 us
  blocking collectives: 0 us -> 1.9 us
    psum x1 -> x0, waiting for transfers between devices: 18.5 us -> none  [per_device(): lax.psum(partial_value.astype(jnp.bfloat16), 'tp').astype(jnp.float32)]
    all_gather x0 -> x1, blocking collectives: none -> 1.9 us  [per_device(): lax.all_gather(partial_value.astype(jnp.bfloat16), 'tp')]
    unnamed x33 -> x31, local copies, waits for them, and re-layouts: 13 us -> 13.7 us
  transfers between devices with their start and end apart: 4 -> 3, of which waited for: 4 -> 3; matrix products, arithmetic and copies ran while one was open for 4% -> 4% of each run, Pallas kernels for 0% -> 0%
where the time goes in v1:
time: 142 us; the launch traced here: 141 us
  waiting for transfers between devices  63.8 us (45%)
  local copies, waits for them, and re-layouts  25.2 us (18%)
  matrix products  17.3 us (12%)
  starting transfers between devices  14.2 us (10%)
  between operations  13.7 us (10%)
  other arithmetic  5.25 us (4%)
  blocking collectives  1.9 us (1%)
    all_to_all x1, waiting for transfers between devices, per_device(): lax.all_to_all(merged, 'ep', split_axis=0, concat_axis=0, tiled=True)  23.9 us
    all_to_all x1, waiting for transfers between devices, per_device(): lax.all_to_all(outgoing, 'ep', split_axis=0, concat_axis=0, tiled=True)  21.3 us
    psum x1, waiting for transfers between devices, per_device(): merged = lax.psum(part_rows.astype(jnp.bfloat16), 'tp')  18.6 us
    unnamed x31, local copies, waits for them, and re-layouts  13.7 us
    all_to_all x1, starting transfers between devices, per_device(): lax.all_to_all(outgoing, 'ep', split_axis=0, concat_axis=0, tiled=True)  7.22 us
    all_to_all x1, starting transfers between devices, per_device(): lax.all_to_all(merged, 'ep', split_axis=0, concat_axis=0, tiled=True)  6.97 us
    dot_general x1, matrix products, attend(): jnp.einsum('skgl,slkd->skgd', past_prob, cached_values, preferred_element...  3.52 us
    dot_general x1, matrix products, attend(): jnp.einsum('skgd,slkd->skgl', queries, cached_keys, preferred_element_typ...  2.98 us
  transfers between devices with their start and end apart: 3, of which 3 were waited for; matrix products, arithmetic and copies ran while one was open for 4% of the time, Pallas kernels for 0%

profile of v1, /device:TPU:8, one launch (start us, length us, event | category | flops | bytes accessed | tf_op | source)
XLA Modules:
  0.0 141.4 jit_solution(14427984710266053740)
XLA Ops:
  6.5 0.7 broadcast_add_fusion
  7.3 0.7 broadcast_compare_fusion
  7.9 0.7 iota_compare_fusion
  8.7 0.8 copy.47
  9.4 0.7 broadcast_multiply_fusion
  10.4 2.0 %gather_fusion.1 = f32[64]{0:T(128)S(1)} fusion(f32[16,4,1024]{2,1,0:T(4,128)} %param.29, s32[64]{0:T(128)S(1)} %reshape.274), kind=kCustom, calls=%fused_computation.1 | custom fusion | bytes 1280 | tf_op jit(solution)/shard_map/jit(take_along_axis)/gather | solution.py:60
  13.5 0.3 convolution_convert_fusion.3
  13.8 6.5 %copy.41 = bf16[16,1024,128]{1,2,0:T(8,128)(2,1)} copy(bf16[16,1024,128]{2,1,0:T(8,128)(2,1)} %param.27) | data formatting | bytes 8388608 | tf_op args[7]
  20.8 3.0 %fusion.55 = (f32[16,2,2]{2,1,0:T(2,128)S(1)}, f32[16,2,2,1024]{3,2,1,0:T(2,128)S(1)}) fusion(f32[16,2,2,1024]{3,2,1,0:T(2,128)S(1)} %reshape.254, bf16[16,2,2,64]{3,2,1,0:T(2,128)(2,1)S(1)} %reshape.252, bf16[16,1024,2,64]{1,3,2,0:T(8,128)(2,1)} %bitcast.51, pred[16,1024]{1,0:T(8,128)(4,1)S(1)} %iota_compare_fusion), kind=kOutput, calls=%fused_computation.103 | convolution fusion | flops 8650688 | bytes 4743424 | tf_op jit(solution)/shard_map/skgd,slkd->skgl/dot_general | solution.py:56
  23.8 0.3 fusion.16
  24.2 0.2 fusion.7
  24.5 6.4 %copy.45 = bf16[16,1024,128]{1,2,0:T(8,128)(2,1)} copy(bf16[16,1024,128]{2,1,0:T(8,128)(2,1)} %param.28) | data formatting | bytes 8388608 | tf_op args[8]
  30.9 3.5 %fusion.2 = bf16[16,2,2,64]{3,2,1,0:T(2,128)(2,1)S(1)} fusion(bf16[16,1024,2,64]{1,3,2,0:T(8,128)(2,1)} %bitcast.52, f32[16,2,2,1024]{3,2,1,0:T(2,128)S(1)} %get-tuple-element.12, f32[16,2,2]{2,1,0:T(2,128)S(1)} %get-tuple-element.8, f32[16,2,2]{2,1,0:T(2,128)S(1)} %multiply_maximum_fusion, f32[16,2,64]{2,1,0:T(2,128)S(1)} %reshape.262, ...), kind=kOutput, calls=%fused_computation.11 | convolution fusion | flops 8597504 | bytes 4473600 | tf_op jit(solution)/shard_map/skgl,slkd->skgd/dot_general | solution.py:75
  34.5 0.3 convolution_convert_fusion.2
  34.8 1.9 %all-gather = bf16[32,2048]{1,0:T(8,128)(2,1)S(1)} all-gather(bf16[16,2048]{1,0:T(8,128)(2,1)S(1)} %convolution_convert_fusion.2), channel_id=2, replica_groups=mesh['ep'=16,'tp'=2] {'tp'}, dimensions={0}, use_global_device_ids=true | all-gather | bytes 196608 | tf_op jit(solution)/shard_map/all_gather | solution.py:117
  37.9 1.4 %scatter_custom_fusion = bf16[192,2048]{1,0:T(8,128)(2,1)S(1)} fusion(s32[96]{0:T(128)S(1)} %fusion.46, bf16[96,2048]{1,0:T(8,128)(2,1)S(1)} %reshape.290, bf16[]{:T(256)} %constant.63.clone.1), kind=kCustom, calls=%fused_computation.29 | custom fusion | bytes 786434 | tf_op jit(solution)/shard_map/scatter | solution.py:135
  39.3 1.2 reshape.259
  40.5 7.2 %all-to-all-start = ((bf16[16,12,2048]{2,1,0:T(8,128)(2,1)}), bf16[16,12,2048]{2,1,0:T(8,128)(2,1)S(1)}, u32[]{:S(2)}, u32[]{:S(2)}) async-start(bf16[16,12,2048]{2,1,0:T(8,128)(2,1)} %reshape.259), calls=%async_computation | async-start | bytes 2097152 | tf_op jit(solution)/shard_map/all_to_all | solution.py:140
  47.7 1.5 %fusion.57 = f32[16,256]{1,0:T(8,128)S(1)} fusion(bf16[16,2048]{1,0:T(8,128)(2,1)S(1)} %fusion.23, bf16[2048,256]{1,0:T(8,128)(2,1)} %param.34), kind=kOutput, calls=%fused_computation.105 | convolution fusion | flops 16777216 | bytes 1130496 | tf_op jit(solution)/shard_map/dot_general | solution.py:18
  49.2 2.9 %convolution_convert_fusion.1 = bf16[16,2048]{1,0:T(8,128)(2,1)} fusion(bf16[256,2048]{1,0:T(8,128)(2,1)} %param.36, bf16[16,2048]{1,0:T(8,128)(2,1)S(1)} %fusion.23, bf16[2048,256]{1,0:T(8,128)(2,1)} %param.35, f32[16,256]{1,0:T(8,128)S(1)} %fusion.57), kind=kOutput, calls=%fused_computation.5 | convolution fusion | flops 33611776 | bytes 2244608 | tf_op jit(solution)/shard_map/dot_general | solution.py:122
  52.1 21.3 %all-to-all-done = bf16[16,12,2048]{2,1,0:T(8,128)(2,1)S(1)} async-done(((bf16[16,12,2048]{2,1,0:T(8,128)(2,1)}), bf16[16,12,2048]{2,1,0:T(8,128)(2,1)S(1)}, u32[]{:S(2)}, u32[]{:S(2)}) %all-to-all-start) | async-done | bytes 786464 | tf_op jit(solution)/shard_map/all_to_all | solution.py:140
  73.5 1.7 %fusion.11 = f32[16,12,256]{2,1,0:T(8,128)S(1)} fusion(bf16[16,12,2048]{2,1,0:T(8,128)(2,1)S(1)} %all-to-all-done, bf16[1,2048,256]{2,1,0:T(8,128)(2,1)} %param.37), kind=kOutput, calls=%fused_computation.26 | convolution fusion | flops 201326592 | bytes 2031616 | tf_op jit(solution)/shard_map/scd,df->scf/dot_general | solution.py:30
  75.1 1.7 %fusion.9 = f32[16,12,256]{2,1,0:T(8,128)S(1)} fusion(bf16[16,12,2048]{2,1,0:T(8,128)(2,1)S(1)} %all-to-all-done, bf16[1,2048,256]{2,1,0:T(8,128)(2,1)} %param.38), kind=kOutput, calls=%fused_computation.24 | convolution fusion | flops 201326592 | bytes 2031616 | tf_op jit(solution)/shard_map/scd,df->scf/dot_general | solution.py:33
  76.8 1.5 %convolution_convert_fusion = bf16[16,12,2048]{2,0,1:T(8,128)(2,1)} fusion(bf16[1,256,2048]{2,1,0:T(8,128)(2,1)S(1)} %copy-done, f32[16,12,256]{2,1,0:T(8,128)S(1)} %fusion.9, f32[16,12,256]{2,1,0:T(8,128)S(1)} %fusion.11), kind=kOutput, calls=%fused_computation.4 | convolution fusion | flops 202014720 | bytes 2228224 | tf_op jit(solution)/shard_map/scf,fd->scd/dot_general | solution.py:144
  78.4 18.6 %all-reduce.3.cloned.1.call-done = (bf16[16,12,2048]{2,0,1:T(8,128)(2,1)}, bf16[16,2048]{1,0:T(8,128)(2,1)}) async-done(((bf16[16,12,2048]{2,0,1:T(8,128)(2,1)}, bf16[16,2048]{1,0:T(8,128)(2,1)}), (bf16[16,12,2048]{2,0,1:T(8,128)(2,1)}, bf16[16,2048]{1,0:T(8,128)(2,1)})) %all-reduce.3.cloned.1.call-update) | async-done | bytes 851984 | tf_op jit(solution)/shard_map/psum | solution.py:147
  97.0 2.6 %copy.50 = bf16[16,12,2048]{2,1,0:T(8,128)(2,1)} copy(bf16[16,12,2048]{2,0,1:T(8,128)(2,1)} %get-tuple-element.5) | data formatting | bytes 1572864 | tf_op jit(solution)/shard_map/psum | solution.py:147
  99.5 7.0 %all-to-all-start.1 = ((bf16[16,12,2048]{2,1,0:T(8,128)(2,1)}), bf16[16,12,2048]{2,1,0:T(8,128)(2,1)S(1)}, u32[]{:S(2)}, u32[]{:S(2)}) async-start(bf16[16,12,2048]{2,1,0:T(8,128)(2,1)} %copy.50), calls=%async_computation.1 | async-start | bytes 2097152 | tf_op jit(solution)/shard_map/all_to_all | solution.py:148
  106.9 1.3 gather_fusion.2
  108.5 23.9 %all-to-all-done.1 = bf16[16,12,2048]{2,1,0:T(8,128)(2,1)S(1)} async-done(((bf16[16,12,2048]{2,1,0:T(8,128)(2,1)}), bf16[16,12,2048]{2,1,0:T(8,128)(2,1)S(1)}, u32[]{:S(2)}, u32[]{:S(2)}) %all-to-all-start.1) | async-done | bytes 786464 | tf_op jit(solution)/shard_map/all_to_all | solution.py:148
  132.5 0.8 gather_fusion
  133.5 0.4 multiply_reduce_fusion
  133.9 0.7 fusion.25
  (78 shorter events, 4.1 us)
Async XLA Ops:
  6.5 70.3 %copy-start = (bf16[1,256,2048]{2,1,0:T(8,128)(2,1)S(1)}, bf16[1,256,2048]{2,1,0:T(8,128)(2,1)}, u32[]{:S(2)}) copy-start(bf16[1,256,2048]{2,1,0:T(8,128)(2,1)} %param.39) | copy-start | bytes 3145732
  10.4 2.3 %copy-start.9 = (bf16[2048]{0:T(1024)(128)(2,1)S(1)}, bf16[2048]{0:T(1024)(128)(2,1)}, u32[]{:S(2)}) copy-start(bf16[2048]{0:T(1024)(128)(2,1)} %param.21) | copy-start | bytes 12292
  10.4 2.3 %copy-start.2 = (bf16[16,2048]{1,0:T(8,128)(2,1)S(1)}, bf16[16,2048]{1,0:T(8,128)(2,1)}, u32[]{:S(2)}) copy-start(bf16[16,2048]{1,0:T(8,128)(2,1)} %param.20) | copy-start | bytes 196612
  10.4 2.4 %copy-start.12 = (bf16[2048,4]{0,1:T(4,128)(2,1)S(1)}, bf16[2048,4]{0,1:T(4,128)(2,1)}, u32[]{:S(2)}) copy-start(bf16[2048,4]{0,1:T(4,128)(2,1)} %param.25) | copy-start | bytes 49156
  10.4 2.7 %copy-start.1 = (f32[16,4,1024]{2,1,0:T(4,128)S(1)}, f32[16,4,1024]{2,1,0:T(4,128)}, u32[]{:S(2)}) copy-start(f32[16,4,1024]{2,1,0:T(4,128)} %param.29) | copy-start | bytes 786436
  10.4 3.0 %copy-start.3 = (bf16[2048,256]{1,0:T(8,128)(2,1)S(1)}, bf16[2048,256]{1,0:T(8,128)(2,1)}, u32[]{:S(2)}) copy-start(bf16[2048,256]{1,0:T(8,128)(2,1)} %param.22) | copy-start | bytes 3145732
  13.8 6.5 %copy-start.5 = (bf16[2048,128]{1,0:T(8,128)(2,1)S(1)}, bf16[2048,128]{1,0:T(8,128)(2,1)}, u32[]{:S(2)}) copy-start(bf16[2048,128]{1,0:T(8,128)(2,1)} %param.23) | copy-start | bytes 1572868
  20.3 3.9 %copy-start.6 = (bf16[2048,128]{1,0:T(8,128)(2,1)S(1)}, bf16[2048,128]{1,0:T(8,128)(2,1)}, u32[]{:S(2)}) copy-start(bf16[2048,128]{1,0:T(8,128)(2,1)} %param.24) | copy-start | bytes 1572868
  30.9 3.6 %copy-start.4 = (bf16[256,2048]{1,0:T(8,128)(2,1)S(1)}, bf16[256,2048]{1,0:T(8,128)(2,1)}, u32[]{:S(2)}) copy-start(bf16[256,2048]{1,0:T(8,128)(2,1)} %param.26) | copy-start | bytes 3145732
  30.9 6.0 %copy-start.10 = (bf16[2048]{0:T(1024)(128)(2,1)S(1)}, bf16[2048]{0:T(1024)(128)(2,1)}, u32[]{:S(2)}) copy-start(bf16[2048]{0:T(1024)(128)(2,1)} %param.31) | copy-start | bytes 12292
  40.5 33.0 %all-to-all-start = ((bf16[16,12,2048]{2,1,0:T(8,128)(2,1)}), bf16[16,12,2048]{2,1,0:T(8,128)(2,1)S(1)}, u32[]{:S(2)}, u32[]{:S(2)}) async-start(bf16[16,12,2048]{2,1,0:T(8,128)(2,1)} %reshape.259), calls=%async_computation | async-start | bytes 2097152 | tf_op jit(solution)/shard_map/all_to_all | solution.py:140
  47.7 49.3 %all-reduce.3.cloned.1.call-start = ((), (), s32[]{:S(2)}) async-start(), calls=%async_computation.2 | async-start | bytes 1703936 | tf_op jit(solution)/shard_map/psum | solution.py:147
  75.1 31.4 %copy-start.7 = (s32[16,6]{0,1:T(8,128)S(1)}, s32[16,6]{0,1:T(8,128)}, u32[]{:S(2)}) copy-start(s32[16,6]{0,1:T(8,128)} %param.33) | copy-start | bytes 1156
  75.1 31.6 %copy-start.11 = (bf16[2048,16]{0,1:T(8,128)(2,1)S(1)}, bf16[2048,16]{0,1:T(8,128)(2,1)}, u32[]{:S(2)}) copy-start(bf16[2048,16]{0,1:T(8,128)(2,1)} %param.32) | copy-start | bytes 196612
  99.5 32.8 %all-to-all-start.1 = ((bf16[16,12,2048]{2,1,0:T(8,128)(2,1)}), bf16[16,12,2048]{2,1,0:T(8,128)(2,1)S(1)}, u32[]{:S(2)}, u32[]{:S(2)}) async-start(bf16[16,12,2048]{2,1,0:T(8,128)(2,1)} %copy.50), calls=%async_computation.1 | async-start | bytes 2097152 | tf_op jit(solution)/shard_map/all_to_all | solution.py:148
  108.2 25.7 %copy-start.8 = (bf16[16,2048]{1,0:T(8,128)(2,1)S(1)}, bf16[16,2048]{1,0:T(8,128)(2,1)}, u32[]{:S(2)}) copy-start(bf16[16,2048]{1,0:T(8,128)(2,1)} %get-tuple-element.6) | copy-start | bytes 196612
Sparse Core Ops, SparseCore 0:
  78.5 18.3 all-reduce.2
